TPU v7x, 512 devices: a 4x2x32 block of a 4x8x32 slice. The times are simulated.
512 devices in a mesh: grp: 2 (over y), sp: 32 (over z), tp: 8 (over x, core).
Axes of the slice: x: 4, y: 2, z: 32, core: 2. Of those that a mesh axis runs over, the one named last changes fastest.
The devices are a block of a 4x8x32 slice.
Arguments:
- latent: bfloat16 [32768, 4096], P(('grp', 'sp', 'tp')), parts along dimension 0, may hold values from -260 to 260
- context: bfloat16 [1536, 4096], P(('grp', 'sp')), parts along dimension 0, may hold values from -6 to 6
- conditioning: bfloat16 [8192], P(('grp', 'sp')), parts along dimension 0, may hold values from -6 to 6
- norm_gain: float32 [4096], replicated, may hold values from 0.1 to 1.9
- shift_weight: bfloat16 [4096, 4096], P('sp', 'tp'), may hold values from -0.09375 to 0.09375
- scale_weight: bfloat16 [4096, 4096], P('sp', 'tp'), may hold values from -0.09375 to 0.09375
- gate_weight: bfloat16 [4096, 4096], P('sp', 'tp'), may hold values from -0.09375 to 0.09375
- query_weight: bfloat16 [4096, 1024], P(None, 'tp'), may hold values from -3 to 3
- key_weight: bfloat16 [4096, 512], P(None, 'tp'), may hold values from -3 to 3
- value_weight: bfloat16 [4096, 512], P(None, 'tp'), may hold values from -0.09375 to 0.09375
- out_weight: bfloat16 [1024, 4096], P(None, 'tp'), may hold values from -1.5 to 1.5
- sink_logit: float32 [16], P('tp'), may hold values from 3 to 7
Outputs:
- mixed: bfloat16 [32768, 4096], P(('grp', 'sp', 'tp')), parts along dimension 0
There are 2 independent parts, one for each index of `grp`. A program takes and returns all parts, laid end to end along the dimension named above; an argument that names none is the same for every part. Nothing has to cross between parts.
All inputs are finite; a program needn't handle non-finite values.
Results may differ from a plain program's by a relative error of at most 0.012.
The roundings to bfloat16 on the way count: a program that leaves them out, or rounds other values in their place, can miss the bound.
Values may be sent and summed in bfloat16 or wider, within the bound.
A program may use at most 64 MiB of HBM per device.

v0:
```python
import jax
import jax.numpy as jnp
from jax import lax
from jax.sharding import PartitionSpec as P

HEADS = 16
KV_HEADS = 8
HD = 64
GRID_W = 64
WIN = 128
epsilon = 1e-06
rope_base = 10000.0
neg_large = -1e30


def sent_to_all(value, axis):
    count = lax.axis_size(axis)
    return lax.all_to_all(
        jnp.broadcast_to(value[None], (count, *value.shape)), axis, 0, 0, tiled=True
    )


def over_copies(value, axis):
    return sent_to_all(value, axis).sum(axis=0)


def packed_total(arrays, axis):
    ends = [0]
    for a in arrays:
        ends.append(ends[-1] + a.size)
    running = over_copies(jnp.concatenate([a.ravel() for a in arrays]), axis)
    return tuple((running[b:e].reshape(a.shape) for a, b, e in zip(arrays, ends, ends[1:])))


def rows_first(arrays, axis, dims):
    turned = [jnp.moveaxis(a, dim, 0) for a, dim in zip(arrays, dims)]
    both = jnp.concatenate([t.reshape(len(t), -1) for t in turned], axis=1)
    whole, at, outs = (lax.all_gather(both, axis, axis=0, tiled=True), 0, [])
    for t, dim in zip(turned, dims):
        share = whole[:, at : at + t[0].size].reshape(-1, *t.shape[1:])
        outs.append(jnp.moveaxis(share, 0, dim))
        at += t[0].size
    return tuple(outs)


def with_halo(cells, sides, width):
    for axis, dim in sides:
        count = lax.axis_size(axis)
        ends = count - 1
        head = lax.slice_in_dim(cells, 0, width, axis=dim)
        tail = lax.slice_in_dim(cells, cells.shape[dim] - width, cells.shape[dim], axis=dim)
        cells = jnp.concatenate(
            [
                lax.ppermute(tail, axis, [(i, (i + 1) % count) for i in range(ends)]),
                cells,
                lax.ppermute(head, axis, [((i + 1) % count, i) for i in range(ends)]),
            ],
            axis=dim,
        )
    return cells


def laid_out(tiles, dim):
    shape = list(tiles.shape[1:])
    shape[dim] *= tiles.shape[0]
    return jnp.moveaxis(tiles, 0, dim).reshape(shape)


def collect(value, axis, dim):
    return laid_out(sent_to_all(value, axis), dim)


def row_norm(matrix, norm_gain):
    values = matrix.astype(jnp.float32)
    return (
        values * lax.rsqrt(jnp.mean(values * values, axis=-1, keepdims=True) + epsilon) * norm_gain
    )


def axial_turn(values, position):
    half_dim = values.shape[-1] // 2
    quarter = half_dim // 2
    inverse = rope_base ** (-jnp.arange(quarter, dtype=jnp.float32) / quarter)

    def turn(section, coordinate):
        angles = coordinate.astype(jnp.float32)[:, None] * inverse[None, :]
        cosine = jnp.cos(angles)[:, None, :]
        sine_part = jnp.sin(angles)[:, None, :]
        leading = section[..., :quarter]
        trailing = section[..., quarter:]
        return jnp.concatenate(
            [leading * cosine - trailing * sine_part, leading * sine_part + trailing * cosine],
            axis=-1,
        )

    return jnp.concatenate(
        [
            turn(values[..., :half_dim], position // GRID_W),
            turn(values[..., half_dim:], position % GRID_W),
        ],
        axis=-1,
    )


def context_pairs(context_rows, norm_gain, key_weight, value_weight):
    prepared = row_norm(context_rows, norm_gain).astype(jnp.bfloat16)
    return jnp.concatenate(
        [
            jnp.dot(prepared, key_weight, preferred_element_type=jnp.float32),
            jnp.dot(prepared, value_weight, preferred_element_type=jnp.float32),
        ],
        axis=1,
    ).astype(jnp.bfloat16)


def local(
    latent,
    context,
    conditioning,
    norm_gain,
    shift_weight,
    scale_weight,
    gate_weight,
    query_weight,
    key_weight,
    value_weight,
    out_weight,
    sink_logit,
):
    lifted = jax.nn.silu(conditioning.astype(jnp.float32)).astype(jnp.bfloat16)[None, :]
    shift_part = jnp.dot(lifted, shift_weight, preferred_element_type=jnp.float32)[0]
    scale_part = jnp.dot(lifted, scale_weight, preferred_element_type=jnp.float32)[0]
    gate_part = jnp.dot(lifted, gate_weight, preferred_element_type=jnp.float32)[0]
    summed = packed_total((shift_part, scale_part, gate_part), "sp")
    shift_vec, scale_vec, gate_vec = rows_first((summed[0], summed[1], summed[2]), "tp", (0, 0, 0))
    normed = (row_norm(latent, norm_gain) * (1.0 + scale_vec) + shift_vec).astype(jnp.bfloat16)
    segment = lax.all_gather(normed, "tp", axis=0, tiled=True)
    projected = jnp.concatenate(
        [
            jnp.dot(segment, query_weight, preferred_element_type=jnp.float32),
            jnp.dot(segment, key_weight, preferred_element_type=jnp.float32),
            jnp.dot(segment, value_weight, preferred_element_type=jnp.float32),
        ],
        axis=1,
    )
    row_count = projected.shape[0]
    query_width = query_weight.shape[1]
    key_width = key_weight.shape[1]
    query_heads = query_width // HD
    pair_heads = key_width // HD
    group_size = HEADS // KV_HEADS
    row_offset = lax.axis_index("sp") * row_count
    position = row_offset + jnp.arange(row_count, dtype=jnp.int32)
    queries = axial_turn(
        projected[:, :query_width].reshape(row_count, query_heads, HD), position
    ).astype(jnp.bfloat16)
    latent_keys = axial_turn(
        projected[:, query_width : query_width + key_width].reshape(row_count, pair_heads, HD),
        position,
    ).astype(jnp.bfloat16)
    latent_values = projected[:, query_width + key_width :].astype(jnp.bfloat16)
    key_value = jnp.concatenate([latent_keys.reshape(row_count, key_width), latent_values], axis=1)
    widened = with_halo(key_value, (("sp", 0),), WIN)
    context_all = collect(context_pairs(context, norm_gain, key_weight, value_weight), "sp", 0)
    block_count = row_count // WIN
    context_count = context_all.shape[0]
    query_blocks = queries.reshape(block_count, WIN, pair_heads, group_size, HD)
    band_blocks = widened.reshape(block_count + 2, WIN, 2 * key_width)
    band_rows = jnp.concatenate(
        [band_blocks[:block_count], band_blocks[1 : block_count + 1], band_blocks[2:]], axis=1
    )
    band_keys = band_rows[..., :key_width].reshape(block_count, 3 * WIN, pair_heads, HD)
    band_values = band_rows[..., key_width:].reshape(block_count, 3 * WIN, pair_heads, HD)
    context_keys = context_all[:, :key_width].reshape(context_count, pair_heads, HD)
    context_values = context_all[:, key_width:].reshape(context_count, pair_heads, HD)
    factor = HD ** (-0.5)
    local_scores = (
        jnp.einsum("nqhgd,nkhd->nhgqk", query_blocks, band_keys, preferred_element_type=jnp.float32)
        * factor
    )
    query_pos = position.reshape(block_count, WIN)
    key_pos = (
        row_offset
        - WIN
        + jnp.arange(block_count, dtype=jnp.int32)[:, None] * WIN
        + jnp.arange(3 * WIN, dtype=jnp.int32)[None, :]
    )
    seq_total = row_count * lax.axis_size("sp")
    allowed = (
        (jnp.abs(key_pos[:, None, :] - query_pos[:, :, None]) <= WIN)
        & (key_pos[:, None, :] >= 0)
        & (key_pos[:, None, :] < seq_total)
    )
    local_scores = jnp.where(allowed[:, None, None], local_scores, neg_large)
    context_scores = (
        jnp.einsum(
            "nqhgd,thd->nhgqt", query_blocks, context_keys, preferred_element_type=jnp.float32
        )
        * factor
    )
    sink_values = sink_logit.reshape(pair_heads, group_size)[None, :, :, None, None]
    highest = jnp.maximum(
        jnp.maximum(
            jnp.max(local_scores, axis=-1, keepdims=True),
            jnp.max(context_scores, axis=-1, keepdims=True),
        ),
        sink_values,
    )
    local_exp = jnp.exp(local_scores - highest)
    context_exp = jnp.exp(context_scores - highest)
    denominator = (
        jnp.sum(local_exp, axis=-1, keepdims=True)
        + jnp.sum(context_exp, axis=-1, keepdims=True)
        + jnp.exp(sink_values - highest)
    )
    local_weights = (local_exp / denominator).astype(jnp.bfloat16)
    context_weights = (context_exp / denominator).astype(jnp.bfloat16)
    attended = jnp.einsum(
        "nhgqk,nkhd->nqhgd", local_weights, band_values, preferred_element_type=jnp.float32
    ) + jnp.einsum(
        "nhgqt,thd->nqhgd", context_weights, context_values, preferred_element_type=jnp.float32
    )
    attended = attended.reshape(row_count, query_width).astype(jnp.bfloat16)
    columns_part = jnp.dot(
        collect(attended, "tp", 1), out_weight, preferred_element_type=jnp.float32
    ).astype(jnp.bfloat16)
    blended = lax.all_to_all(columns_part, "tp", split_axis=0, concat_axis=1, tiled=True)
    return (latent.astype(jnp.float32) + gate_vec * blended.astype(jnp.float32)).astype(
        jnp.bfloat16
    )


def solution(mesh):
    in_specs = (
        P(("grp", "sp", "tp"), None),
        P(("grp", "sp"), None),
        P(("grp", "sp")),
        P(),
        P("sp", "tp"),
        P("sp", "tp"),
        P("sp", "tp"),
        P(None, "tp"),
        P(None, "tp"),
        P(None, "tp"),
        P(None, "tp"),
        P("tp"),
    )
    out_specs = P(("grp", "sp", "tp"), None)
    return jax.shard_map(local, mesh=mesh, in_specs=in_specs, out_specs=out_specs, check_vma=False)
```

profile of v0, /device:TPU:33, one launch (start us, length us, event | category | flops | bytes accessed | tf_op | source)
XLA Modules:
  0.0 197.6 jit_solution(16965403692785830598)
XLA Ops:
  6.5 0.0 copy-start
  6.6 1.2 fusion.60
  7.8 1.1 fusion.58
  8.8 1.1 fusion.56
  9.9 0.8 broadcast_in_dim.14
  10.7 46.3 %all-to-all-start = ((f32[32,1,1536]{2,1,0:T(1,128)}), f32[32,1,1536]{2,1,0:T(1,128)S(1)}, u32[]{:S(2)}, u32[]{:S(2)}) async-start(f32[32,1,1536]{2,1,0:T(1,128)} %broadcast_in_dim.14), calls=%async_computation | async-start | bytes 393216 | tf_op jit(solution)/shard_map/all_to_all | solution.py:18
  57.0 0.1 all-gather.2.cloned.1.call-start
  57.1 1.2 fusion.12
  58.3 33.6 %all-to-all-done = f32[32,1,1536]{2,1,0:T(1,128)S(1)} async-done(((f32[32,1,1536]{2,1,0:T(1,128)}), f32[32,1,1536]{2,1,0:T(1,128)S(1)}, u32[]{:S(2)}, u32[]{:S(2)}) %all-to-all-start) | async-done | bytes 196640 | tf_op jit(solution)/shard_map/all_to_all | solution.py:18
  91.9 0.1 reduce_sum.45
  92.0 15.7 %all_gather.6 = f32[4096,3]{0,1:T(4,128)S(1)} all-gather(f32[512,3]{0,1:T(4,128)S(1)} %pad_maximum_fusion.3), channel_id=1, replica_groups=mesh['grp'=2,'sp'=32,'tp'=8] {'tp'}, dimensions={0}, use_global_device_ids=true | all-gather | bytes 55296 | tf_op jit(solution)/shard_map/all_gather | solution.py:38
  107.8 2.1 %fusion.16 = bf16[64,4096]{1,0:T(8,128)(2,1)} fusion(bf16[64,4096]{1,0:T(8,128)(2,1)} %param.12, f32[4096]{0:T(1024)S(1)} %bitcast.164, f32[4096]{0:T(1024)S(1)} %bitcast.165, f32[4096]{0:T(1024)} %param.15, f32[64]{0:T(128)S(1)} %add_rsqrt_fusion.1), kind=kLoop, calls=%fused_computation.29 | loop fusion | flops 1572864 | bytes 1097984 | tf_op jit(solution)/shard_map/convert_element_type | solution.py:136
  109.9 0.1 all-gather.2.cloned.1.call-update
  110.0 0.0 copy-done.5
  110.0 0.2 fusion.21
  110.2 0.0 copy-done.7
  110.2 0.0 copy-done.4
  110.2 0.3 convolution_convert_fusion.2
  110.5 0.0 copy-done.3
  110.5 0.3 convolution_convert_fusion.3
  110.8 0.1 pad_maximum_fusion.4
  110.9 0.7 broadcast_in_dim.17
  111.6 4.8 %all-to-all-start.1 = ((bf16[32,24,128]{2,1,0:T(8,128)(2,1)}), bf16[32,24,128]{2,1,0:T(8,128)(2,1)S(1)}, u32[]{:S(2)}, u32[]{:S(2)}) async-start(bf16[32,24,128]{2,1,0:T(8,128)(2,1)} %broadcast_in_dim.17), calls=%async_computation.1 | async-start | bytes 393216 | tf_op jit(solution)/shard_map/all_to_all | solution.py:18
  116.5 0.1 fusion.50
  116.5 0.1 iota_add_fusion
  116.6 0.3 multiply_cosine_fusion
  116.9 0.9 fusion.20
  117.9 21.9 %all-gather.2.cloned.1.call-done = bf16[512,4096]{1,0:T(8,128)(2,1)} async-done(((bf16[64,4096]{1,0:T(8,128)(2,1)}), bf16[512,4096]{1,0:T(8,128)(2,1)}) %all-gather.2.cloned.1.call-update) | async-done | bytes 4194320 | tf_op jit(solution)/shard_map/all_gather | solution.py:137
  139.8 3.7 %convolution_bitcast_fusion.1 = f32[512,1,64]{0,2,1:T(8,128)S(1)} fusion(bf16[512,4096]{1,0:T(8,128)(2,1)} %all-gather.2.cloned.1.call-done, bf16[4096,64]{0,1:T(8,128)(2,1)S(1)} %copy-done.3), kind=kOutput, calls=%fused_computation.20 | convolution fusion | flops 268435456 | bytes 4849664 | tf_op jit(solution)/shard_map/dot_general | solution.py:141
  143.5 0.0 copy-start.6
  143.5 0.2 constant_dynamic-update-slice_fusion.3
  143.7 0.2 constant_dynamic-update-slice_fusion.2
  143.9 0.2 constant_dynamic-update-slice_fusion.1
  144.1 0.2 constant_dynamic-update-slice_fusion
  144.3 0.0 copy-done.1
  144.3 1.4 fusion.11
  145.7 1.3 collective-permute-start.1
  147.0 4.2 %collective-permute-start = (bf16[128,128]{0,1:T(8,128)(2,1)S(1)}, bf16[128,128]{0,1:T(8,128)(2,1)S(1)}, u32[]{:S(2)}, u32[]{:S(2)}) collective-permute-start(bf16[128,128]{0,1:T(8,128)(2,1)S(1)} %get-tuple-element.14), channel_id=1, source_target_pairs={{0,8},{8,16},{16,24},{24,32},{32,40},{40,48},{48,56},{56,64},{64,7... | collective-permute-start | bytes 98312 | tf_op jit(solution)/shard_map/ppermute | solution.py:54
  151.2 0.0 copy-done.6
  151.3 1.5 fusion.70
  152.9 0.0 all-to-all-done.1
  152.9 0.0 copy-start.8
  152.9 0.6 bitcast_reduce_fusion
  153.5 0.0 collective-permute-done.1
  153.5 0.0 collective-permute-done
  153.7 0.4 fusion.69
  154.1 0.0 copy-done.8
  154.1 0.1 maximum_maximum_fusion
  154.2 0.5 fusion.1
  154.8 0.2 fusion.5
  155.0 0.1 exponential_add_fusion
  155.1 0.8 fusion.7
  155.9 0.4 fusion.10
  156.3 0.1 copy.58
  156.4 0.1 broadcast_in_dim.18
  156.5 19.3 %all_to_all.29 = bf16[8,512,128]{1,2,0:T(8,128)(2,1)S(1)} all-to-all(bf16[8,512,128]{1,2,0:T(8,128)(2,1)S(1)} %broadcast_in_dim.18), channel_id=1, replica_groups=mesh['grp'=2,'sp'=32,'tp'=8] {'tp'}, dimensions={0} | all-to-all | bytes 2097152 | tf_op jit(solution)/shard_map/all_to_all | solution.py:18
  175.9 0.0 copy-done
  175.9 0.7 convolution_convert_fusion
  176.6 0.0 copy-start.2
  176.6 13.0 %all_to_all.30 = bf16[8,64,512]{2,1,0:T(8,128)(2,1)S(1)} all-to-all(bf16[8,64,512]{2,1,0:T(8,128)(2,1)S(1)} %bitcast.161), channel_id=1, replica_groups=mesh['grp'=2,'sp'=32,'tp'=8] {'tp'}, dimensions={0} | all-to-all | bytes 1048576 | tf_op jit(solution)/shard_map/all_to_all | solution.py:227
  189.6 0.1 convert_bitcast_fusion
  189.7 0.1 copy.79
  189.8 0.0 copy-done.2
  189.8 0.9 fusion.17
  (26 shorter events, 0.4 us)
Async XLA Ops:
  6.5 169.3 %copy-start = (bf16[1024,512]{1,0:T(8,128)(2,1)S(1)}, bf16[1024,512]{1,0:T(8,128)(2,1)}, u32[]{:S(2)}) copy-start(bf16[1024,512]{1,0:T(8,128)(2,1)} %param.22) | copy-start | bytes 3145732
  6.6 103.6 %copy-start.7 = (f32[4096]{0:T(1024)S(1)}, f32[4096]{0:T(1024)}, u32[]{:S(2)}) copy-start(f32[4096]{0:T(1024)} %param.15) | copy-start | bytes 49156
  6.6 103.4 %copy-start.5 = (bf16[24,4096]{1,0:T(8,128)(2,1)S(1)}, bf16[24,4096]{1,0:T(8,128)(2,1)}, u32[]{:S(2)}) copy-start(bf16[24,4096]{1,0:T(8,128)(2,1)} %param.13) | copy-start | bytes 589828
  6.6 103.6 %copy-start.4 = (bf16[4096,64]{0,1:T(8,128)(2,1)S(1)}, bf16[4096,64]{0,1:T(8,128)(2,1)}, u32[]{:S(2)}) copy-start(bf16[4096,64]{0,1:T(8,128)(2,1)} %param.21) | copy-start | bytes 1572868
  6.6 103.9 %copy-start.3 = (bf16[4096,64]{0,1:T(8,128)(2,1)S(1)}, bf16[4096,64]{0,1:T(8,128)(2,1)}, u32[]{:S(2)}) copy-start(bf16[4096,64]{0,1:T(8,128)(2,1)} %param.20) | copy-start | bytes 1572868
  10.7 81.2 %all-to-all-start = ((f32[32,1,1536]{2,1,0:T(1,128)}), f32[32,1,1536]{2,1,0:T(1,128)S(1)}, u32[]{:S(2)}, u32[]{:S(2)}) async-start(f32[32,1,1536]{2,1,0:T(1,128)} %broadcast_in_dim.14), calls=%async_computation | async-start | bytes 393216 | tf_op jit(solution)/shard_map/all_to_all | solution.py:18
  57.0 82.8 %all-gather.2.cloned.1.call-start = ((), (), s32[]{:S(2)}) async-start(), calls=%async_computation.4 | async-start | bytes 4718592 | tf_op jit(solution)/shard_map/all_gather | solution.py:137
  111.6 41.3 %all-to-all-start.1 = ((bf16[32,24,128]{2,1,0:T(8,128)(2,1)}), bf16[32,24,128]{2,1,0:T(8,128)(2,1)S(1)}, u32[]{:S(2)}, u32[]{:S(2)}) async-start(bf16[32,24,128]{2,1,0:T(8,128)(2,1)} %broadcast_in_dim.17), calls=%async_computation.1 | async-start | bytes 393216 | tf_op jit(solution)/shard_map/all_to_all | solution.py:18
  139.8 4.5 %copy-start.1 = (bf16[512,4096]{1,0:T(8,128)(2,1)S(1)}, bf16[512,4096]{1,0:T(8,128)(2,1)}, u32[]{:S(2)}) copy-start(bf16[512,4096]{1,0:T(8,128)(2,1)} %all-gather.2.cloned.1.call-done) | copy-start | bytes 12582916
  143.5 7.8 %copy-start.6 = (bf16[4096,128]{1,0:T(8,128)(2,1)S(1)}, bf16[4096,128]{1,0:T(8,128)(2,1)}, u32[]{:S(2)}) copy-start(bf16[4096,128]{1,0:T(8,128)(2,1)} %param.19) | copy-start | bytes 3145732
  145.7 7.8 %collective-permute-start.1 = (bf16[128,128]{0,1:T(8,128)(2,1)S(1)}, bf16[128,128]{0,1:T(8,128)(2,1)S(1)}, u32[]{:S(2)}, u32[]{:S(2)}) collective-permute-start(bf16[128,128]{0,1:T(8,128)(2,1)S(1)} %get-tuple-element.13), channel_id=1, source_target_pairs={{8,0},{16,8},{24,16},{32,24},{40,32},{48,40},{56,48},{64,56},{72,6... | collective-permute-start | bytes 98312 | tf_op jit(solution)/shard_map/ppermute | solution.py:56
  147.0 6.5 %collective-permute-start = (bf16[128,128]{0,1:T(8,128)(2,1)S(1)}, bf16[128,128]{0,1:T(8,128)(2,1)S(1)}, u32[]{:S(2)}, u32[]{:S(2)}) collective-permute-start(bf16[128,128]{0,1:T(8,128)(2,1)S(1)} %get-tuple-element.14), channel_id=1, source_target_pairs={{0,8},{8,16},{16,24},{24,32},{32,40},{40,48},{48,56},{56,64},{64,7... | collective-permute-start | bytes 98312 | tf_op jit(solution)/shard_map/ppermute | solution.py:54
  152.9 1.2 copy-start.8
  176.6 13.2 %copy-start.2 = (bf16[64,4096]{1,0:T(8,128)(2,1)S(1)}, bf16[64,4096]{1,0:T(8,128)(2,1)}, u32[]{:S(2)}) copy-start(bf16[64,4096]{1,0:T(8,128)(2,1)} %param.12) | copy-start | bytes 1572868
Sparse Core Ops, SparseCore 0:
  110.1 29.6 all-gather.1
where the time goes:
time: 198 us
  starting transfers between devices  56.7 us (29%)
  waiting for transfers between devices  55.5 us (28%)
  blocking collectives  48 us (24%)
  between operations  13.8 us (7%)
  matrix products  13.5 us (7%)
  other arithmetic  8.05 us (4%)
  local copies, waits for them, and re-layouts  2.02 us (1%)
    all_to_all x2, starting transfers between devices, sent_to_all(): lax.all_to_all(jnp.broadcast_to(value[None], (count, *value.shape)), axis...  51.1 us
    all_to_all x2, waiting for transfers between devices, sent_to_all(): lax.all_to_all(jnp.broadcast_to(value[None], (count, *value.shape)), axis...  33.6 us
    all_gather x1, waiting for transfers between devices, local(): segment = lax.all_gather(normed, 'tp', axis=0, tiled=True)  21.9 us
    all_to_all x1, blocking collectives, sent_to_all(): lax.all_to_all(jnp.broadcast_to(value[None], (count, *value.shape)), axis...  19.3 us
    all_gather x1, blocking collectives, rows_first(): whole, at, outs = (lax.all_gather(both, axis, axis=0, tiled=True), 0, [])  15.7 us
    all_to_all x1, blocking collectives, local(): lax.all_to_all(columns_part, 'tp', split_axis=0, concat_axis=1, tiled=True)  13 us
    ppermute x1, starting transfers between devices, with_halo(): lax.ppermute(tail, axis, [(i, (i + 1) % count) for i in range(ends)])  4.21 us
  transfers between devices with their start and end apart: 5, of which 2 were waited for; matrix products, arithmetic and copies ran while one was open for 6% of the time, Pallas kernels for 0%

commit v1 on v0

--- a/solution.py
+++ b/solution.py
@@ -11,6 +11,14 @@
 epsilon = 1e-06
 rope_base = 10000.0
 neg_large = -1e30
+
+
+def tiled_gather(value, axis, dim):
+    devices = lax.axis_size(axis)
+    repeats = [devices if d == dim else 1 for d in range(value.ndim)]
+    return lax.all_to_all(
+        jnp.tile(value, repeats), axis, split_axis=dim, concat_axis=dim, tiled=True
+    )
 
 
 def sent_to_all(value, axis):
@@ -134,7 +142,7 @@
     summed = packed_total((shift_part, scale_part, gate_part), "sp")
     shift_vec, scale_vec, gate_vec = rows_first((summed[0], summed[1], summed[2]), "tp", (0, 0, 0))
     normed = (row_norm(latent, norm_gain) * (1.0 + scale_vec) + shift_vec).astype(jnp.bfloat16)
-    segment = lax.all_gather(normed, "tp", axis=0, tiled=True)
+    segment = tiled_gather(normed, "tp", 0)
     projected = jnp.concatenate(
         [
             jnp.dot(segment, query_weight, preferred_element_type=jnp.float32),

time: 198 us -> 238 us (1.20)
  waiting for transfers between devices: 55.5 us -> 97.3 us
  between operations: 13.8 us -> 0.37 us
  matrix products: 13.5 us -> 17.7 us
  local copies, waits for them, and re-layouts: 2.02 us -> 5.89 us
  starting transfers between devices: 56.7 us -> 59.7 us
    all_to_all x0 -> x1, waiting for transfers between devices: none -> 45.1 us  [tiled_gather(): lax.all_to_all(jnp.tile(value, repeats), axis, split_axis=dim, concat_axi...]
    all_gather x1 -> x0, waiting for transfers between devices: 21.9 us -> none  [local(): segment = lax.all_gather(normed, 'tp', axis=0, tiled=True)]
    all_to_all x2, waiting for transfers between devices: 33.6 us -> 52.2 us  [sent_to_all(): lax.all_to_all(jnp.broadcast_to(value[None], (count, *value.shape)), axis...]
    all_to_all x0 -> x1, starting transfers between devices: none -> 4.75 us  [tiled_gather(): lax.all_to_all(jnp.tile(value, repeats), axis, split_axis=dim, concat_axi...]
    another operation x0 -> x1, local copies, waits for them, and re-layouts: none -> 2.5 us  [tiled_gather(): jnp.tile(value, repeats)]
  transfers between devices with their start and end apart: 5 -> 5, of which waited for: 2 -> 3; matrix products, arithmetic and copies ran while one was open for 6% -> 7% of each run, Pallas kernels for 0% -> 0%
where the time goes in v1:
time: 238 us
  waiting for transfers between devices  97.3 us (41%)
  starting transfers between devices  59.7 us (25%)
  blocking collectives  49.4 us (21%)
  matrix products  17.7 us (7%)
  other arithmetic  7.25 us (3%)
  local copies, waits for them, and re-layouts  5.89 us (2%)
    all_to_all x2, waiting for transfers between devices, sent_to_all(): lax.all_to_all(jnp.broadcast_to(value[None], (count, *value.shape)), axis...  52.2 us
    all_to_all x2, starting transfers between devices, sent_to_all(): lax.all_to_all(jnp.broadcast_to(value[None], (count, *value.shape)), axis...  51.1 us
    all_to_all x1, waiting for transfers between devices, tiled_gather(): lax.all_to_all(jnp.tile(value, repeats), axis, split_axis=dim, concat_axi...  45.1 us
    all_to_all x1, blocking collectives, sent_to_all(): lax.all_to_all(jnp.broadcast_to(value[None], (count, *value.shape)), axis...  20.7 us
    all_gather x1, blocking collectives, rows_first(): whole, at, outs = (lax.all_gather(both, axis, axis=0, tiled=True), 0, [])  15.7 us
    all_to_all x1, blocking collectives, local(): lax.all_to_all(columns_part, 'tp', split_axis=0, concat_axis=1, tiled=True)  13 us
  transfers between devices with their start and end apart: 5, of which 3 were waited for; matrix products, arithmetic and copies ran while one was open for 7% of the time, Pallas kernels for 0%

profile of v1, /device:TPU:33, one launch (start us, length us, event | category | flops | bytes accessed | tf_op | source)
XLA Modules:
  0.0 237.6 jit_solution(15978489735749285395)
XLA Ops:
  0.0 0.0 copy-start
  0.0 1.1 fusion.60
  1.1 1.1 fusion.58
  2.2 1.1 fusion.56
  3.3 0.8 broadcast_in_dim.14
  4.1 46.3 %all-to-all-start = ((f32[32,1,1536]{2,1,0:T(1,128)}), f32[32,1,1536]{2,1,0:T(1,128)S(1)}, u32[]{:S(2)}, u32[]{:S(2)}) async-start(f32[32,1,1536]{2,1,0:T(1,128)} %broadcast_in_dim.14), calls=%async_computation | async-start | bytes 393216 | tf_op jit(solution)/shard_map/all_to_all | solution.py:26
  50.4 1.2 fusion.12
  51.6 33.6 %all-to-all-done = f32[32,1,1536]{2,1,0:T(1,128)S(1)} async-done(((f32[32,1,1536]{2,1,0:T(1,128)}), f32[32,1,1536]{2,1,0:T(1,128)S(1)}, u32[]{:S(2)}, u32[]{:S(2)}) %all-to-all-start) | async-done | bytes 196640 | tf_op jit(solution)/shard_map/all_to_all | solution.py:26
  85.3 0.1 reduce_sum.45
  85.4 15.7 %all_gather.3 = f32[4096,3]{0,1:T(4,128)S(1)} all-gather(f32[512,3]{0,1:T(4,128)S(1)} %pad_maximum_fusion.3), channel_id=1, replica_groups=mesh['grp'=2,'sp'=32,'tp'=8] {'tp'}, dimensions={0}, use_global_device_ids=true | all-gather | bytes 55296 | tf_op jit(solution)/shard_map/all_gather | solution.py:46
  101.2 1.3 fusion.16
  102.5 2.5 %tile.2 = bf16[8,64,4096]{2,1,0:T(8,128)(2,1)} broadcast(bf16[64,4096]{1,0:T(8,128)(2,1)S(1)} %fusion.16), dimensions={1,2} | broadcast | bytes 4718592 | tf_op jit(solution)/shard_map/tile | solution.py:20
  105.0 0.0 copy-start.2
  105.0 4.8 %all-to-all-start.1 = ((bf16[8,64,4096]{2,1,0:T(8,128)(2,1)}), bf16[8,64,4096]{2,1,0:T(8,128)(2,1)}, u32[]{:S(2)}, u32[]{:S(2)}) async-start(bf16[8,64,4096]{2,1,0:T(8,128)(2,1)} %tile.2), calls=%async_computation.1 | async-start | bytes 8388608 | tf_op jit(solution)/shard_map/all_to_all | solution.py:19
  109.8 0.0 copy-done.5
  109.8 1.4 copy.57
  111.2 0.0 copy-done.4
  111.2 0.2 fusion.21
  111.4 0.0 copy-done.3
  111.4 0.0 copy-done.7
  111.4 0.3 convolution_convert_fusion.2
  111.7 0.0 copy-done.2
  111.7 0.3 convolution_convert_fusion.3
  112.1 0.1 pad_maximum_fusion.4
  112.1 0.1 fusion.50
  112.2 0.1 iota_add_fusion
  112.3 0.3 multiply_cosine_fusion
  112.6 0.9 fusion.20
  113.6 45.1 %all-to-all-done.1 = bf16[8,64,4096]{2,1,0:T(8,128)(2,1)} async-done(((bf16[8,64,4096]{2,1,0:T(8,128)(2,1)}), bf16[8,64,4096]{2,1,0:T(8,128)(2,1)}, u32[]{:S(2)}, u32[]{:S(2)}) %all-to-all-start.1) | async-done | bytes 4194336 | tf_op jit(solution)/shard_map/all_to_all | solution.py:19
  158.7 0.7 broadcast_in_dim.17
  159.4 4.8 %all-to-all-start.2 = ((bf16[32,24,128]{2,1,0:T(8,128)(2,1)}), bf16[32,24,128]{2,1,0:T(8,128)(2,1)S(1)}, u32[]{:S(2)}, u32[]{:S(2)}) async-start(bf16[32,24,128]{2,1,0:T(8,128)(2,1)} %broadcast_in_dim.17), calls=%async_computation.2 | async-start | bytes 393216 | tf_op jit(solution)/shard_map/all_to_all | solution.py:26
  164.1 3.6 %convolution_bitcast_fusion.1 = f32[512,1,64]{0,2,1:T(8,128)S(1)} fusion(bf16[512,4096]{1,0:T(8,128)(2,1)} %bitcast.12, bf16[4096,64]{0,1:T(8,128)(2,1)S(1)} %copy-done.2), kind=kOutput, calls=%fused_computation.20 | convolution fusion | flops 268435456 | bytes 4849664 | tf_op jit(solution)/shard_map/dot_general | solution.py:149
  167.7 0.2 constant_dynamic-update-slice_fusion.3
  167.9 0.2 constant_dynamic-update-slice_fusion.2
  168.1 0.2 constant_dynamic-update-slice_fusion.1
  168.3 0.2 constant_dynamic-update-slice_fusion
  168.5 3.6 %fusion.11 = bf16[512,128]{0,1:T(8,128)(2,1)S(1)} fusion(bf16[512,128]{0,1:T(8,128)(2,1)S(1)} %constant_dynamic-update-slice_fusion, bf16[512,4096]{1,0:T(8,128)(2,1)} %bitcast.12, bf16[4096,64]{0,1:T(8,128)(2,1)S(1)} %copy-done.3), kind=kOutput, calls=%fused_computation.22 | convolution fusion | flops 268468224 | bytes 4784128 | tf_op jit(solution)/shard_map/dot_general | solution.py:150
  172.1 2.4 collective-permute-start
  174.5 1.5 collective-permute-start.1
  176.0 0.0 copy-done.6
  176.0 3.7 %fusion.70 = f32[512,2,64]{0,2,1:T(8,128)S(1)} fusion(bf16[512,4096,1]{1,0,2:T(8,128)(2,1)} %bitcast.22, bf16[2,64,4096]{2,1,0:T(8,128)(2,1)S(1)} %bitcast.161), kind=kOutput, calls=%fused_computation.135 | convolution fusion | flops 536870912 | bytes 5505024 | tf_op jit(solution)/shard_map/dot_general | solution.py:148
  179.9 18.6 %all-to-all-done.2 = bf16[32,24,128]{2,1,0:T(8,128)(2,1)S(1)} async-done(((bf16[32,24,128]{2,1,0:T(8,128)(2,1)}), bf16[32,24,128]{2,1,0:T(8,128)(2,1)S(1)}, u32[]{:S(2)}, u32[]{:S(2)}) %all-to-all-start.2) | async-done | bytes 196640 | tf_op jit(solution)/shard_map/all_to_all | solution.py:26
  198.4 0.6 bitcast_reduce_fusion
  199.0 0.0 collective-permute-done
  199.0 0.0 collective-permute-done.1
  199.2 0.4 fusion.69
  199.6 0.0 copy-done.8
  199.6 0.1 maximum_maximum_fusion
  199.7 0.5 fusion.1
  200.2 0.2 fusion.5
  200.5 0.1 exponential_add_fusion
  200.6 0.8 fusion.7
  201.4 0.4 fusion.10
  201.8 0.1 copy.66
  201.9 0.1 broadcast_in_dim.18
  202.0 20.7 %all_to_all.38 = bf16[8,512,128]{1,2,0:T(8,128)(2,1)S(1)} all-to-all(bf16[8,512,128]{1,2,0:T(8,128)(2,1)S(1)} %broadcast_in_dim.18), channel_id=1, replica_groups=mesh['grp'=2,'sp'=32,'tp'=8] {'tp'}, dimensions={0} | all-to-all | bytes 2097152 | tf_op jit(solution)/shard_map/all_to_all | solution.py:26
  222.7 0.0 copy-done
  222.7 0.7 convolution_convert_fusion
  223.4 0.0 copy-start.1
  223.5 13.0 %all_to_all.39 = bf16[8,64,512]{2,1,0:T(8,128)(2,1)S(1)} all-to-all(bf16[8,64,512]{2,1,0:T(8,128)(2,1)S(1)} %bitcast.166), channel_id=1, replica_groups=mesh['grp'=2,'sp'=32,'tp'=8] {'tp'}, dimensions={0} | all-to-all | bytes 1048576 | tf_op jit(solution)/shard_map/all_to_all | solution.py:235
  236.4 0.1 convert_bitcast_fusion
  236.6 0.1 copy.87
  236.7 0.0 copy-done.1
  236.7 0.9 fusion.17
  (27 shorter events, 0.4 us)
Async XLA Ops:
  0.0 222.7 %copy-start = (bf16[1024,512]{1,0:T(8,128)(2,1)S(1)}, bf16[1024,512]{1,0:T(8,128)(2,1)}, u32[]{:S(2)}) copy-start(bf16[1024,512]{1,0:T(8,128)(2,1)} %param.22) | copy-start | bytes 3145732
  4.1 81.2 %all-to-all-start = ((f32[32,1,1536]{2,1,0:T(1,128)}), f32[32,1,1536]{2,1,0:T(1,128)S(1)}, u32[]{:S(2)}, u32[]{:S(2)}) async-start(f32[32,1,1536]{2,1,0:T(1,128)} %broadcast_in_dim.14), calls=%async_computation | async-start | bytes 393216 | tf_op jit(solution)/shard_map/all_to_all | solution.py:26
  105.0 4.8 %copy-start.5 = (bf16[4096,128]{1,0:T(8,128)(2,1)S(1)}, bf16[4096,128]{1,0:T(8,128)(2,1)}, u32[]{:S(2)}) copy-start(bf16[4096,128]{1,0:T(8,128)(2,1)} %param.19) | copy-start | bytes 3145732
  105.0 6.2 %copy-start.4 = (bf16[24,4096]{1,0:T(8,128)(2,1)S(1)}, bf16[24,4096]{1,0:T(8,128)(2,1)}, u32[]{:S(2)}) copy-start(bf16[24,4096]{1,0:T(8,128)(2,1)} %param.13) | copy-start | bytes 589828
  105.0 6.4 %copy-start.3 = (bf16[4096,64]{0,1:T(8,128)(2,1)S(1)}, bf16[4096,64]{0,1:T(8,128)(2,1)}, u32[]{:S(2)}) copy-start(bf16[4096,64]{0,1:T(8,128)(2,1)} %param.21) | copy-start | bytes 1572868
  105.0 6.4 %copy-start.7 = (f32[4096]{0:T(1024)S(1)}, f32[4096]{0:T(1024)}, u32[]{:S(2)}) copy-start(f32[4096]{0:T(1024)} %param.15) | copy-start | bytes 49156
  105.0 6.7 %copy-start.2 = (bf16[4096,64]{0,1:T(8,128)(2,1)S(1)}, bf16[4096,64]{0,1:T(8,128)(2,1)}, u32[]{:S(2)}) copy-start(bf16[4096,64]{0,1:T(8,128)(2,1)} %param.20) | copy-start | bytes 1572868
  105.0 53.6 %all-to-all-start.1 = ((bf16[8,64,4096]{2,1,0:T(8,128)(2,1)}), bf16[8,64,4096]{2,1,0:T(8,128)(2,1)}, u32[]{:S(2)}, u32[]{:S(2)}) async-start(bf16[8,64,4096]{2,1,0:T(8,128)(2,1)} %tile.2), calls=%async_computation.1 | async-start | bytes 8388608 | tf_op jit(solution)/shard_map/all_to_all | solution.py:19
  159.4 39.1 %all-to-all-start.2 = ((bf16[32,24,128]{2,1,0:T(8,128)(2,1)}), bf16[32,24,128]{2,1,0:T(8,128)(2,1)S(1)}, u32[]{:S(2)}, u32[]{:S(2)}) async-start(bf16[32,24,128]{2,1,0:T(8,128)(2,1)} %broadcast_in_dim.17), calls=%async_computation.2 | async-start | bytes 393216 | tf_op jit(solution)/shard_map/all_to_all | solution.py:26
  167.7 8.3 %copy-start.6 = (bf16[4096,128]{0,1:T(8,128)(2,1)S(1)}, bf16[4096,128]{0,1:T(8,128)(2,1)}, u32[]{:S(2)}) copy-start(bf16[4096,128]{0,1:T(8,128)(2,1)} %copy.57) | copy-start | bytes 3145732
  172.1 26.9 %collective-permute-start = (bf16[128,128]{0,1:T(8,128)(2,1)S(1)}, bf16[128,128]{0,1:T(8,128)(2,1)S(1)}, u32[]{:S(2)}, u32[]{:S(2)}) collective-permute-start(bf16[128,128]{0,1:T(8,128)(2,1)S(1)} %get-tuple-element.14), channel_id=1, source_target_pairs={{0,8},{8,16},{16,24},{24,32},{32,40},{40,48},{48,56},{56,64},{64,7... | collective-permute-start | bytes 98312 | tf_op jit(solution)/shard_map/ppermute | solution.py:62
  174.5 24.5 %collective-permute-start.1 = (bf16[128,128]{0,1:T(8,128)(2,1)S(1)}, bf16[128,128]{0,1:T(8,128)(2,1)S(1)}, u32[]{:S(2)}, u32[]{:S(2)}) collective-permute-start(bf16[128,128]{0,1:T(8,128)(2,1)S(1)} %get-tuple-element.13), channel_id=1, source_target_pairs={{8,0},{16,8},{24,16},{32,24},{40,32},{48,40},{56,48},{64,56},{72,6... | collective-permute-start | bytes 98312 | tf_op jit(solution)/shard_map/ppermute | solution.py:64
  198.4 1.2 copy-start.8
  223.4 13.2 %copy-start.1 = (bf16[64,4096]{1,0:T(8,128)(2,1)S(1)}, bf16[64,4096]{1,0:T(8,128)(2,1)}, u32[]{:S(2)}) copy-start(bf16[64,4096]{1,0:T(8,128)(2,1)} %param.12) | copy-start | bytes 1572868
